TPU v7x, 32 devices: a whole 2x2x4 slice. The times are simulated.
32 devices in a mesh: ep: 8 (over z, x), tp: 4 (over y, core).
Axes of the slice: x: 2, y: 2, z: 4, core: 2. Of those that a mesh axis runs over, the one named last changes fastest.
Arguments:
- query_rows: bfloat16 [1536, 1024], P('ep', 'tp'), may hold values from -8 to 8
- key_rows: bfloat16 [1536, 1024], P('ep', 'tp'), may hold values from -8 to 8
- value_rows: bfloat16 [1536, 1024], P('ep', 'tp'), may hold values from -6 to 6
- lambdas: float32 [8], P('tp'), may hold values from 0.3 to 0.8
- head_gain: float32 [128], replicated, may hold values from 0.1 to 1.9
- w_out: bfloat16 [1024, 2048], replicated, may hold values from -0.1875 to 0.1875
- moe_rows: bfloat16 [4096, 2048], P('ep'), may hold values from -6 to 6
- ffn_gain: float32 [2048], replicated, may hold values from 0.1 to 1.9
- routes: int32 [4096, 2], P('ep'), may hold values from 0 to 7, all different within a row; in each aligned block of 128 rows (0 to 127, 128 to 255, ...) at most 64 rows name the same one
- group_logits: float32 [4096, 4], P('ep'), may hold values from -8 to 8
- pick_logits: float32 [4096, 2], P('ep'), may hold values from -8 to 8
- w_gate: bfloat16 [8, 2048, 1024], P('ep', None, 'tp'), may hold values from -0.125 to 0.125
- w_up: bfloat16 [8, 2048, 1024], P('ep', None, 'tp'), may hold values from -0.125 to 0.125
- w_down: bfloat16 [8, 1024, 2048], P('ep', 'tp'), may hold values from -0.75 to 0.75
Outputs:
- mixer_out: bfloat16 [1536, 2048], P(('ep', 'tp'))
- moe_out: bfloat16 [4096, 2048], P(('ep', 'tp'))
Inputs may be any that keep to these rules, and one draw needn't show every extreme that they name: `routes`: each row names 2 different experts. In each aligned block of 128 rows (the rows of one device) no expert is named by more than 64 rows; some expert is named by exactly 64 rows of a block.
All inputs are finite; a program needn't handle non-finite values.
Results may differ from a plain program's by a relative error of at most 0.015.
Values may be sent and summed in bfloat16 or wider, within the bound.
A program may use at most 128 MiB of HBM per device.

v0:
```python
import jax
import jax.numpy as jnp
from jax import lax
from jax.sharding import PartitionSpec as P

EPS = 1e-06
HEAD_SCALE = 0.8


def rms_rows(values, gain):
    squared = jnp.mean(values * values, axis=-1, keepdims=True)
    return values * lax.rsqrt(squared + EPS) * gain


def slot_index(picks, expert_count, capacity):
    flattened = picks.reshape(picks.shape[0], -1)
    onehot = (flattened[..., None] == jnp.arange(expert_count, dtype=jnp.int32)).astype(jnp.int32)
    before = jnp.cumsum(onehot, axis=1) - onehot
    ranking = jnp.sum(before * onehot, axis=-1)
    return flattened * capacity + ranking


def expert_hidden(arrived, gate_weight, up_weight):
    gate_part = jnp.dot(arrived, gate_weight, preferred_element_type=jnp.float32)
    up_part = jnp.dot(arrived, up_weight, preferred_element_type=jnp.float32)
    return (jax.nn.silu(gate_part) * up_part).astype(jnp.bfloat16)


def local(
    query_rows,
    key_rows,
    value_rows,
    lambdas,
    head_gain,
    w_out,
    moe_rows,
    ffn_gain,
    routes,
    group_logits,
    pick_logits,
    w_gate,
    w_up,
    w_down,
):
    token_count = query_rows.shape[0]
    local_heads = lambdas.shape[0]
    head_qk = query_rows.shape[1] // (2 * local_heads)
    head_v = value_rows.shape[1] // local_heads
    score_scale = head_qk ** (-0.5)
    queries = query_rows.reshape(token_count, local_heads, 2, head_qk)

    def absorb(carried, key_value):
        key_block, value_block = key_value
        running_max, running_sum, running_acc = carried
        scores = (
            jnp.einsum("qhmd,khmd->hmqk", queries, key_block, preferred_element_type=jnp.float32)
            * score_scale
        )
        new_max = jnp.maximum(running_max, jnp.max(scores, axis=-1))
        factor = jnp.exp(running_max - new_max)
        weights = jnp.exp(scores - new_max[..., None])
        running_sum = running_sum * factor + jnp.sum(weights, axis=-1)
        update = jnp.einsum(
            "hmqk,khv->hmqv",
            weights.astype(jnp.bfloat16),
            value_block,
            preferred_element_type=jnp.float32,
        )
        return ((new_max, running_sum, running_acc * factor[..., None] + update), None)

    start_state = (
        jnp.full((local_heads, 2, token_count), -1e30, jnp.float32),
        jnp.zeros((local_heads, 2, token_count), jnp.float32),
        jnp.zeros((local_heads, 2, token_count, head_v), jnp.float32),
    )
    carried = start_state
    key_piece = lax.all_gather(key_rows, "ep", axis=0, tiled=True)
    value_piece = lax.all_gather(value_rows, "ep", axis=0, tiled=True)
    length = key_piece.shape[0]
    block_rows = 1024 if length % 1024 == 0 else length
    blocks = (
        key_piece.reshape(length // block_rows, block_rows, local_heads, 2, head_qk),
        value_piece.reshape(length // block_rows, block_rows, local_heads, head_v),
    )
    carried, unused = lax.scan(absorb, carried, blocks)
    unused_max, final_sum, final_acc = carried
    averaged = final_acc / final_sum[..., None]
    per_head = averaged[:, 0] - lambdas[:, None, None] * averaged[:, 1]
    normed_heads = rms_rows(per_head, head_gain) * HEAD_SCALE
    attended = (
        jnp.transpose(normed_heads, (1, 0, 2))
        .reshape(token_count, local_heads * head_v)
        .astype(jnp.bfloat16)
    )
    own_weight = lax.dynamic_slice_in_dim(
        w_out, lax.axis_index("tp") * attended.shape[1], attended.shape[1], 0
    )
    mixer_out = lax.psum_scatter(
        jnp.dot(attended, own_weight, preferred_element_type=jnp.float32).astype(jnp.bfloat16),
        "tp",
        scatter_dimension=0,
        tiled=True,
    )
    quarters = lax.axis_size("tp")
    own_quarter = lax.axis_index("tp")
    expert_count = lax.axis_size("ep")
    model_width = moe_rows.shape[1]
    quarter_rows = moe_rows.shape[0] // quarters
    top_k = routes.shape[1]
    capacity = max(2, 2 * top_k * quarter_rows // expert_count)
    source_rows = jnp.repeat(jnp.arange(quarter_rows, dtype=jnp.int32), top_k)
    own_picks = lax.dynamic_slice_in_dim(routes, own_quarter * quarter_rows, quarter_rows, 0)
    own_tokens = lax.dynamic_slice_in_dim(moe_rows, own_quarter * quarter_rows, quarter_rows, 0)
    normed = rms_rows(own_tokens.astype(jnp.float32), ffn_gain).astype(jnp.bfloat16)
    own_slots = slot_index(own_picks[None], expert_count, capacity)[0]
    outgoing = (
        jnp.zeros((expert_count * capacity, model_width), jnp.bfloat16)
        .at[own_slots]
        .set(normed[source_rows])
    )
    arrived = lax.all_to_all(
        outgoing.reshape(expert_count, capacity, model_width),
        "ep",
        split_axis=0,
        concat_axis=0,
        tiled=True,
    )
    pieces = lax.all_gather(arrived, "tp", axis=0, tiled=True)
    flat_rows = pieces.reshape(-1, model_width)
    hidden = expert_hidden(flat_rows, w_gate[0], w_up[0]).reshape(pieces.shape[0], capacity, -1)
    hidden_flat = hidden.reshape(-1, hidden.shape[-1])
    summed = lax.psum_scatter(
        jnp.dot(hidden_flat, w_down[0], preferred_element_type=jnp.float32).astype(jnp.bfloat16),
        "tp",
        scatter_dimension=0,
        tiled=True,
    )
    returned = lax.all_to_all(
        summed.reshape(expert_count, capacity, model_width),
        "ep",
        split_axis=0,
        concat_axis=0,
        tiled=True,
    )
    picked = returned.reshape(-1, model_width)[own_slots].reshape(quarter_rows, top_k, model_width)
    own_groups = lax.dynamic_slice_in_dim(group_logits, own_quarter * quarter_rows, quarter_rows, 0)
    own_pick_logits = lax.dynamic_slice_in_dim(
        pick_logits, own_quarter * quarter_rows, quarter_rows, 0
    )
    group_count = group_logits.shape[1]
    group_prob = jax.nn.softmax(own_groups, axis=-1)
    group_index = own_picks // (expert_count // group_count)
    matches = (group_index[..., None] == jnp.arange(group_count, dtype=jnp.int32)).astype(
        jnp.float32
    )
    group_share = jnp.sum(group_prob[:, None, :] * matches, axis=-1)
    gate_values = group_share * jax.nn.softmax(own_pick_logits, axis=-1)
    moe_out = jnp.sum(gate_values[..., None] * picked.astype(jnp.float32), axis=1).astype(
        jnp.bfloat16
    )
    return (mixer_out, moe_out)


def solution(mesh):
    return jax.shard_map(
        local,
        mesh=mesh,
        in_specs=(
            P("ep", "tp"),
            P("ep", "tp"),
            P("ep", "tp"),
            P("tp"),
            P(),
            P(),
            P("ep", None),
            P(),
            P("ep", None),
            P("ep", None),
            P("ep", None),
            P("ep", None, "tp"),
            P("ep", None, "tp"),
            P("ep", "tp", None),
        ),
        out_specs=(P(("ep", "tp"), None), P(("ep", "tp"), None)),
        check_vma=False,
    )
```

profile of v0, /device:TPU:0, one launch (start us, length us, event | category | flops | bytes accessed | tf_op | source)
XLA Modules:
  0.0 339.7 jit_solution(261808291416860606)
XLA Ops:
  7.2 0.0 copy-start
  7.2 0.0 all-gather.2.cloned.1.call-start
  7.2 0.8 and_select_fusion
  8.0 0.1 copy.52
  8.1 0.1 eq.43
  8.3 0.6 reduce-window.6
  8.9 0.2 slice_reduce_fusion
  9.1 0.1 fusion.32
  9.2 0.1 copy.51
  9.3 0.1 mul.152
  9.5 0.1 reshape.255
  9.6 1.2 fusion.10
  10.9 2.0 fusion.12
  12.9 6.2 %scatter_custom_fusion = bf16[512,2048]{1,0:T(8,128)(2,1)S(1)} fusion(s32[256]{0:T(256)S(1)} %bitcast.82, bf16[128,2048]{1,0:T(8,128)(2,1)} %fusion.12, s32[1024]{0:T(1024)S(1)} %pad_clamp_fusion.1, bf16[]{:T(256)} %constant.73.clone.1), kind=kCustom, calls=%fused_computation.25 | custom fusion | bytes 2097664 | tf_op jit(solution)/shard_map/scatter | solution.py:119
  19.2 55.4 %all_to_all.10 = bf16[8,64,2048]{2,1,0:T(8,128)(2,1)} all-to-all(bf16[8,64,2048]{2,1,0:T(8,128)(2,1)S(1)} %bitcast.77), channel_id=1, replica_groups=mesh['ep'=8,'tp'=4] {'ep'}, dimensions={0} | all-to-all | bytes 4194304 | tf_op jit(solution)/shard_map/all_to_all | solution.py:121
  74.6 0.0 all-gather.2.cloned.1.call-update
  74.6 0.2 reduce-scatter.5.cloned.1.call-start
  74.9 57.2 %all-gather.2.cloned.1.call-done = bf16[32,64,2048]{2,1,0:T(8,128)(2,1)} async-done(((bf16[8,64,2048]{2,1,0:T(8,128)(2,1)}), bf16[32,64,2048]{2,1,0:T(8,128)(2,1)}) %all-gather.2.cloned.1.call-update) | async-done | bytes 8388624 | tf_op jit(solution)/shard_map/all_gather | solution.py:128
  132.1 0.0 copy-start.9
  132.1 7.4 %fusion.16 = f32[2048,256]{1,0:T(8,128)} fusion(bf16[2048,2048]{1,0:T(8,128)(2,1)} %bitcast.87, bf16[1,2048,256]{2,1,0:T(8,128)(2,1)} %param.25), kind=kOutput, calls=%fused_computation.23 | convolution fusion | flops 2147483648 | bytes 11534336 | tf_op jit(solution)/shard_map/dot_general | solution.py:24
  139.5 0.0 copy-done
  139.5 0.0 copy-done.9
  139.5 13.2 %convolution_convert_fusion = bf16[2048,2048]{1,0:T(8,128)(2,1)} fusion(bf16[2048,2048]{1,0:T(8,128)(2,1)} %bitcast.88, f32[2048,256]{1,0:T(8,128)} %fusion.16, bf16[1,256,2048]{2,1,0:T(8,128)(2,1)S(1)} %copy-done, bf16[1,2048,256]{2,1,0:T(8,128)(2,1)S(1)} %copy-done.9), kind=kOutput, calls=%fused_computation.3 | convolution fusion | flops 4302307328 | bytes 20971520 | tf_op jit(solution)/shard_map/dot_general | solution.py:133
  152.7 0.0 copy-start.2
  152.7 0.0 reduce-scatter.5.cloned.1.call-update
  152.7 0.9 copy-done.2
  153.5 0.0 copy-start.3
  153.6 32.4 %all_gather.9 = bf16[1536,256]{1,0:T(8,128)(2,1)S(1)} all-gather(bf16[192,256]{1,0:T(8,128)(2,1)S(1)} %copy-done.2), channel_id=1, replica_groups=mesh['ep'=8,'tp'=4] {'ep'}, dimensions={0}, use_global_device_ids=true | all-gather | bytes 884736 | tf_op jit(solution)/shard_map/all_gather | solution.py:77
  186.0 1.2 copy.45
  187.1 0.0 copy-done.3
  187.1 0.0 copy-start.4
  187.1 0.1 copy.44
  187.2 37.0 %reduce-scatter.5.cloned.1.call-done = bf16[512,2048]{1,0:T(8,128)(2,1)} async-done(((bf16[2048,2048]{1,0:T(8,128)(2,1)}), bf16[512,2048]{1,0:T(8,128)(2,1)}) %reduce-scatter.5.cloned.1.call-update) | async-done | bytes 2097168 | tf_op jit(solution)/shard_map/reduce_scatter | solution.py:132
  224.2 5.5 %all-to-all-start.1 = ((bf16[8,64,2048]{2,1,0:T(8,128)(2,1)}), bf16[8,64,2048]{2,1,0:T(8,128)(2,1)S(1)}, u32[]{:S(2)}, u32[]{:S(2)}) async-start(bf16[8,64,2048]{2,1,0:T(8,128)(2,1)} %bitcast.79), calls=%async_computation.3 | async-start | bytes 4194304 | tf_op jit(solution)/shard_map/all_to_all | solution.py:138
  229.7 0.0 reduce-scatter.3.cloned.1.call-start
  229.8 0.0 copy-done.4
  229.8 71.9 %all_gather.10 = bf16[1536,256]{1,0:T(8,128)(2,1)} all-gather(bf16[192,256]{1,0:T(8,128)(2,1)S(1)} %copy-done.4), channel_id=1, replica_groups=mesh['ep'=8,'tp'=4] {'ep'}, dimensions={0}, use_global_device_ids=true | all-gather | bytes 884736 | tf_op jit(solution)/shard_map/all_gather | solution.py:78
  301.7 2.3 copy.46
  304.0 2.0 multiply_reduce_fusion
  306.1 0.0 copy-start.1
  306.1 0.9 fusion
  307.0 0.2 copy-done.1
  307.2 0.0 copy-start.7
  307.2 0.0 copy-start.8
  307.2 1.2 fusion.23
  308.4 0.0 copy-done.7
  308.4 0.0 copy-start.5
  308.4 0.0 copy-start.6
  308.5 0.2 multiply_reduce_fusion.2
  308.7 0.0 copy-done.8
  308.7 2.6 convolution_convert_fusion.1
  311.3 0.0 reduce-scatter.3.cloned.1.call-update
  311.3 0.0 copy-done.5
  311.3 0.0 copy-done.6
  311.5 0.1 copy.50
  311.6 0.0 all-to-all-done.1
  311.6 2.3 gather_fusion
  314.0 2.4 reshape.260
  316.4 3.9 %multiply_reduce_fusion.1 = bf16[128,2048]{1,0:T(8,128)(2,1)} fusion(f32[128,2,2048]{2,1,0:T(2,128)S(1)} %reshape.260, f32[128,2]{1,0:T(8,128)S(1)} %copy.50), kind=kLoop, calls=%fused_computation.14 | loop fusion | flops 786432 | bytes 2622464 | tf_op jit(solution)/shard_map/reduce_sum | solution.py:158
  320.3 12.9 %reduce-scatter.3.cloned.1.call-done = bf16[48,2048]{1,0:T(8,128)(2,1)} async-done(((bf16[192,2048]{1,0:T(8,128)(2,1)}), bf16[48,2048]{1,0:T(8,128)(2,1)}) %reduce-scatter.3.cloned.1.call-update) | async-done | bytes 196624 | tf_op jit(solution)/shard_map/reduce_scatter | solution.py:98
  (19 shorter events, 0.3 us)
Async XLA Ops:
  7.2 132.3 %copy-start = (bf16[1,256,2048]{2,1,0:T(8,128)(2,1)S(1)}, bf16[1,256,2048]{2,1,0:T(8,128)(2,1)}, u32[]{:S(2)}) copy-start(bf16[1,256,2048]{2,1,0:T(8,128)(2,1)} %param.27) | copy-start | bytes 3145732
  7.2 124.9 %all-gather.2.cloned.1.call-start = ((), (), s32[]{:S(2)}) async-start(), calls=%async_computation.5 | async-start | bytes 10485760 | tf_op jit(solution)/shard_map/all_gather | solution.py:128
  74.6 149.6 %reduce-scatter.5.cloned.1.call-start = ((), (), s32[]{:S(2)}) async-start(), calls=%async_computation.6 | async-start | bytes 10485760 | tf_op jit(solution)/shard_map/reduce_scatter | solution.py:132
  132.1 7.4 %copy-start.9 = (bf16[1,2048,256]{2,1,0:T(8,128)(2,1)S(1)}, bf16[1,2048,256]{2,1,0:T(8,128)(2,1)}, u32[]{:S(2)}) copy-start(bf16[1,2048,256]{2,1,0:T(8,128)(2,1)} %param.26) | copy-start | bytes 3145732
  152.7 0.9 copy-start.2
  153.5 33.6 %copy-start.3 = (bf16[192,256]{1,0:T(8,128)(2,1)S(1)}, bf16[192,256]{1,0:T(8,128)(2,1)}, u32[]{:S(2)}) copy-start(bf16[192,256]{1,0:T(8,128)(2,1)} %param.14) | copy-start | bytes 294916
  187.1 42.6 %copy-start.4 = (bf16[192,256]{1,0:T(8,128)(2,1)S(1)}, bf16[192,256]{1,0:T(8,128)(2,1)}, u32[]{:S(2)}) copy-start(bf16[192,256]{1,0:T(8,128)(2,1)} %param.16) | copy-start | bytes 294916
  224.2 87.4 %all-to-all-start.1 = ((bf16[8,64,2048]{2,1,0:T(8,128)(2,1)}), bf16[8,64,2048]{2,1,0:T(8,128)(2,1)S(1)}, u32[]{:S(2)}, u32[]{:S(2)}) async-start(bf16[8,64,2048]{2,1,0:T(8,128)(2,1)} %bitcast.79), calls=%async_computation.3 | async-start | bytes 4194304 | tf_op jit(solution)/shard_map/all_to_all | solution.py:138
  229.7 103.5 %reduce-scatter.3.cloned.1.call-start = ((), (), s32[]{:S(2)}) async-start(), calls=%async_computation.4 | async-start | bytes 983040 | tf_op jit(solution)/shard_map/reduce_scatter | solution.py:98
  306.1 1.1 copy-start.1
  307.2 1.2 copy-start.7
  307.2 1.5 copy-start.8
  308.4 2.9 copy-start.5
  308.4 2.9 copy-start.6
Sparse Core Ops, SparseCore 0:
  74.7 57.2 all-gather.1
  152.8 71.3 reduce-scatter.4
  311.4 21.7 reduce-scatter.2
where the time goes:
time: 340 us
  blocking collectives  160 us (47%)
  waiting for transfers between devices  107 us (31%)
  matrix products  26.4 us (8%)
  local copies, waits for them, and re-layouts  16.6 us (5%)
  between operations  14 us (4%)
  other arithmetic  10 us (3%)
  starting transfers between devices  5.81 us (2%)
    all_gather x1, blocking collectives, local(): value_piece = lax.all_gather(value_rows, 'ep', axis=0, tiled=True)  71.9 us
    all_gather x1, waiting for transfers between devices, local(): pieces = lax.all_gather(arrived, 'tp', axis=0, tiled=True)  57.2 us
    all_to_all x1, blocking collectives, local(): lax.all_to_all(outgoing.reshape(expert_count, capacity, model_width), 'ep...  55.4 us
    reduce_scatter x1, waiting for transfers between devices, local(): lax.psum_scatter(jnp.dot(hidden_flat, w_down[0], preferred_element_type=j...  37 us
    all_gather x1, blocking collectives, local(): key_piece = lax.all_gather(key_rows, 'ep', axis=0, tiled=True)  32.4 us
    dot_general x1, matrix products, local(): jnp.dot(hidden_flat, w_down[0], preferred_element_type=jnp.float32)  13.2 us
    reduce_scatter x1, waiting for transfers between devices, local(): lax.psum_scatter(jnp.dot(attended, own_weight, preferred_element_type=jnp...  12.9 us
    dot_general x1, matrix products, expert_hidden(): jnp.dot(arrived, gate_weight, preferred_element_type=jnp.float32)  7.4 us
  transfers between devices with their start and end apart: 4, of which 3 were waited for; matrix products, arithmetic and copies ran while one was open for 6% of the time, Pallas kernels for 0%

commit v1 on v0

v1 whole, which is shorter than its diff:
```python
import functools

import jax
import jax.numpy as jnp
from jax import lax
from jax.experimental import pallas as pl
from jax.experimental.pallas import tpu as pltpu
from jax.sharding import PartitionSpec as P

EPS = 1e-06
HEAD_SCALE = 0.8
CHUNKS = 4
MESH = pl.DeviceIdType.MESH
F32 = jnp.float32
BF16 = jnp.bfloat16


def flat_rows(values):
    blocks, rows, columns = values.shape
    if rows % 16:
        return values.astype(F32).reshape(blocks * rows, columns).astype(values.dtype)
    return values.reshape(blocks * rows, columns)


def split_rows(values, rows):
    columns = values.shape[1]
    if rows % 16:
        return values.reshape(-1, rows, columns).astype(BF16)
    return values.astype(BF16).reshape(-1, rows, columns)


def kernel(
    n,
    tp,
    dims,
    query_ref,
    key_ref,
    value_ref,
    lambda_ref,
    head_gain_ref,
    w_out_ref,
    moe_ref,
    ffn_gain_ref,
    routes_ref,
    groups_ref,
    picks_ref,
    gate_ref,
    up_ref,
    down_ref,
    mixer_ref,
    out_ref,
    rows_buf,
    sent,
    arrived,
    w_gate,
    w_up,
    w_down,
    keys,
    values,
    w_out,
    attended,
    collected,
    hidden,
    results,
    returned,
    local_sem,
    weight_send,
    weight_recv,
    row_send,
    row_recv,
    kv_send,
    kv_recv,
    back_send,
    back_recv,
    head_send,
    head_recv,
):
    token_count, local_heads, head_qk, head_v, quarter, capacity, group_count = dims
    ep = lax.axis_index("ep")
    me = lax.axis_index("tp")
    mate = me + 1 - 2 * lax.rem(me, 2)
    across = lax.rem(me + tp // 2, tp)
    diagonal = lax.rem(mate + tp // 2, tp)
    beside = ep + 1 - 2 * lax.rem(ep, 2)
    half = n // 2
    width = out_ref.shape[1]
    part = width // CHUNKS

    def remote(source, target, send, recv, device):
        return pltpu.make_async_remote_copy(
            src_ref=source,
            dst_ref=target,
            send_sem=send,
            recv_sem=recv,
            device_id=device,
            device_id_type=MESH,
        )

    own_rows = pltpu.make_async_copy(
        moe_ref.at[pl.ds(pl.multiple_of(me * quarter, quarter), quarter)], rows_buf, local_sem.at[0]
    )
    own_rows.start()
    locals_ = [
        pltpu.make_async_copy(gate_ref.at[0], w_gate.at[0], local_sem.at[1]),
        pltpu.make_async_copy(up_ref.at[0], w_up.at[0], local_sem.at[2]),
        pltpu.make_async_copy(down_ref.at[0], w_down.at[0], local_sem.at[3]),
        pltpu.make_async_copy(key_ref, keys.at[0], local_sem.at[4]),
        pltpu.make_async_copy(value_ref, values.at[0], local_sem.at[5]),
        pltpu.make_async_copy(w_out_ref, w_out, local_sem.at[6]),
    ]
    for copy in locals_:
        copy.start()

    barrier = pltpu.get_barrier_semaphore()
    for peer in (mate, across, diagonal):
        pl.semaphore_signal(barrier, inc=1, device_id=(ep, peer), device_id_type=MESH)

    def greet(step, carry):
        pl.semaphore_signal(
            barrier, inc=1, device_id=(lax.rem(ep + step, n), me), device_id_type=MESH
        )
        return carry

    lax.fori_loop(1, n, greet, 0)
    pl.semaphore_wait(barrier, n - 1 + 3)

    def columns(number):
        return pl.ds(number * part, part)

    def weight_copies(place, first):
        device = (ep, across if place == 2 else mate)
        sources = (
            (gate_ref.at[0], up_ref.at[0], down_ref.at[0])
            if first
            else (w_gate.at[2], w_up.at[2], w_down.at[2])
        )
        base = place - 1
        copies = [
            remote(
                sources[0],
                w_gate.at[place],
                weight_send.at[base, 0],
                weight_recv.at[base, 0],
                device,
            ),
            remote(
                sources[1],
                w_up.at[place],
                weight_send.at[base, 1],
                weight_recv.at[base, 1],
                device,
            ),
        ]
        for number in range(CHUNKS):
            copies.append(
                remote(
                    sources[2].at[:, columns(number)],
                    w_down.at[place, :, columns(number)],
                    weight_send.at[base, 2 + number],
                    weight_recv.at[base, 2 + number],
                    device,
                )
            )
        return copies

    to_across = weight_copies(2, True)
    to_mate = weight_copies(1, True)
    relayed = weight_copies(3, False)
    for copy in to_across:
        copy.start()
    for copy in to_mate:
        copy.start()

    own = pl.ds(pl.multiple_of(me * quarter, quarter), quarter)
    routes = routes_ref[own, :]
    first, second = routes[:, 0:1], routes[:, 1:2]
    lanes = lax.broadcasted_iota(jnp.int32, (quarter, 128), 1)
    away = [lax.rem(pick - ep + n, n) for pick in (first, second)]
    named = jnp.where((lanes == away[0]) | (lanes == away[1]), 1.0, 0.0)
    row_at = lax.broadcasted_iota(jnp.int32, (quarter, quarter), 0)
    column_at = lax.broadcasted_iota(jnp.int32, (quarter, quarter), 1)
    earlier = jnp.where(column_at < row_at, 1.0, 0.0).astype(BF16)
    before = jnp.dot(earlier, named.astype(BF16), preferred_element_type=F32)
    places = [
        away_k * capacity
        + jnp.sum(jnp.where(lanes == away_k, before, 0.0), axis=1, keepdims=True).astype(jnp.int32)
        for away_k in away
    ]
    slot_at = lax.broadcasted_iota(jnp.int32, (quarter, n * capacity), 1)
    pick_of = [jnp.where(slot_at == place, 1.0, 0.0) for place in places]
    spread = (pick_of[0] + pick_of[1]).astype(BF16)

    own_rows.wait()
    tokens = rows_buf[...].astype(F32)
    squared = jnp.mean(tokens * tokens, axis=-1, keepdims=True)
    normed = (tokens * lax.rsqrt(squared + EPS) * ffn_gain_ref[...]).astype(BF16)
    slotted = lax.dot_general(
        spread, normed, (((0,), (0,)), ((), ())), preferred_element_type=F32
    )
    sent[...] = split_rows(slotted, capacity)

    def row_copy(step):
        return remote(
            sent.at[step],
            arrived.at[step],
            row_send.at[step],
            row_recv.at[step],
            (lax.rem(ep + step, n), me),
        )

    def start_rows(step, carry):
        row_copy(step).start()
        return carry

    lax.fori_loop(1, n, start_rows, 0)
    arrived[0] = sent[0]

    def kv_copies(step, relay):
        to = step + half if relay else step
        device = (beside, me) if relay else (lax.rem(ep + 2 * step, n), me)
        key_source = keys.at[step] if relay else key_ref
        value_source = values.at[step] if relay else value_ref
        return (
            remote(key_source, keys.at[to], kv_send.at[0, to], kv_recv.at[0, to], device),
            remote(value_source, values.at[to], kv_send.at[1, to], kv_recv.at[1, to], device),
        )

    def start_kv(step, carry):
        for copy in kv_copies(step, False):
            copy.start()
        return carry

    lax.fori_loop(1, half, start_kv, 0)

    groups = groups_ref[own, :]
    group_weights = jnp.exp(groups - jnp.max(groups, axis=-1, keepdims=True))
    group_prob = group_weights / jnp.sum(group_weights, axis=-1, keepdims=True)
    picks = picks_ref[own, :]
    pick_weights = jnp.exp(picks - jnp.max(picks, axis=-1, keepdims=True))
    pick_prob = pick_weights / jnp.sum(pick_weights, axis=-1, keepdims=True)
    group_at = lax.broadcasted_iota(jnp.int32, groups.shape, 1)
    gates = [
        jnp.sum(jnp.where(group_at == pick // (n // group_count), group_prob, 0.0), axis=1, keepdims=True)
        * pick_prob[:, k : k + 1]
        for k, pick in enumerate((first, second))
    ]

    for copy in locals_:
        copy.wait()

    to_across[0].wait_recv()
    relayed[0].start()

    def wait_rows(step, carry):
        row_copy(step).wait_recv()
        return carry

    lax.fori_loop(1, n, wait_rows, 0)
    units = gate_ref.shape[2]

    def hide(place):
        rows = flat_rows(arrived[...])
        gate_part = jnp.dot(rows, w_gate[place], preferred_element_type=F32)
        up_part = jnp.dot(rows, w_up[place], preferred_element_type=F32)
        hidden[place] = (gate_part / (1.0 + jnp.exp(-gate_part)) * up_part).astype(BF16)

    hide(0)
    to_mate[0].wait_recv()
    to_mate[1].wait_recv()
    hide(1)
    to_across[1].wait_recv()
    relayed[1].start()
    hide(2)
    relayed[0].wait_recv()
    relayed[1].wait_recv()
    hide(3)

    def back_copy(number, step):
        return remote(
            results.at[number, step],
            returned.at[number, step],
            back_send.at[number, step],
            back_recv.at[number, step],
            (lax.rem(ep - step + n, n), me),
        )

    for number in range(CHUNKS):
        to_across[2 + number].wait_recv()
        relayed[2 + number].start()
        to_mate[2 + number].wait_recv()
        total = jnp.zeros((n * capacity, part), F32)
        for place in range(3):
            total += jnp.dot(
                hidden[place], w_down[place, :, columns(number)], preferred_element_type=F32
            )
        relayed[2 + number].wait_recv()
        total += jnp.dot(hidden[3], w_down[3, :, columns(number)], preferred_element_type=F32)
        results[number] = split_rows(total, capacity)

        def start_back(step, carry):
            back_copy(number, step).start()
            return carry

        lax.fori_loop(1, n, start_back, 0)
        returned[number, 0] = results[number, 0]

    def relay_kv(step, carry):
        for copy in kv_copies(step, False):
            copy.wait_recv()
        for copy in kv_copies(step, True):
            copy.start()
        return carry

    for copy in kv_copies(0, True):
        copy.start()
    lax.fori_loop(1, half, relay_kv, 0)

    def wait_kv(step, carry):
        for copy in kv_copies(step, True):
            copy.wait_recv()
        return carry

    lax.fori_loop(0, half, wait_kv, 0)

    blocks = min(n, 8)
    scale = head_qk**-0.5
    share = token_count // tp
    for head in range(local_heads):
        averaged = []
        for way in range(2):
            at = (2 * head + way) * head_qk
            query = query_ref[:, at : at + head_qk]

            def scored(step):
                key_rows = keys[pl.ds(step * blocks, blocks), :, at : at + head_qk]
                return (
                    lax.dot_general(
                        query,
                        key_rows.reshape(blocks * token_count, head_qk),
                        (((1,), (1,)), ((), ())),
                        preferred_element_type=F32,
                    )
                    * scale
                )

            def absorb(step, carry):
                top, mass, sums = carry
                scores = scored(step)
                new_top = jnp.maximum(top, jnp.max(scores, axis=-1, keepdims=True))
                factor = jnp.exp(top - new_top)
                weights = jnp.exp(scores - new_top)
                value_rows = values[
                    pl.ds(step * blocks, blocks), :, head * head_v : (head + 1) * head_v
                ].reshape(blocks * token_count, head_v)
                mass = mass * factor + jnp.sum(weights, axis=-1, keepdims=True)
                sums = sums * factor + jnp.dot(
                    weights.astype(BF16), value_rows, preferred_element_type=F32
                )
                return new_top, mass, sums

            start = (
                jnp.full((token_count, 1), -1e30, F32),
                jnp.zeros((token_count, 1), F32),
                jnp.zeros((token_count, head_v), F32),
            )
            if n == blocks:
                top, mass, sums = absorb(0, start)
            else:
                top, mass, sums = lax.fori_loop(0, n // blocks, absorb, start)
            averaged.append(sums / mass)
        lambda_at = lambda_ref[0, head]
        per_head = averaged[0] - lambda_at * averaged[1]
        squares = jnp.mean(per_head * per_head, axis=-1, keepdims=True)
        normed_head = per_head * lax.rsqrt(squares + EPS) * head_gain_ref[...] * HEAD_SCALE
        attended[:, :, head * head_v : (head + 1) * head_v] = normed_head.astype(BF16).reshape(
            tp, share, head_v
        )

    head_copies = []
    for step in range(1, tp):
        head_copies.append(
            remote(
                attended.at[lax.rem(me + step, tp)],
                collected.at[step],
                head_send.at[step],
                head_recv.at[step],
                (ep, lax.rem(me + step, tp)),
            )
        )
    for copy in head_copies:
        copy.start()
    collected[0] = attended[me]
    depth = local_heads * head_v
    for copy in head_copies:
        copy.wait_recv()
    mixed = jnp.zeros((share, width), F32)
    for step in range(tp):
        from_tp = lax.rem(me - step + tp, tp)
        mixed += jnp.dot(
            collected[step],
            w_out[pl.ds(pl.multiple_of(from_tp * depth, depth), depth), :],
            preferred_element_type=F32,
        )
    mixer_ref[...] = mixed.astype(BF16)

    choose = [pick.astype(BF16) for pick in pick_of]
    for number in range(CHUNKS):

        def wait_back(step, carry):
            back_copy(number, step).wait_recv()
            return carry

        lax.fori_loop(1, n, wait_back, 0)
        rows = flat_rows(returned[number])
        combined = gates[0] * jnp.dot(choose[0], rows, preferred_element_type=F32)
        combined += gates[1] * jnp.dot(choose[1], rows, preferred_element_type=F32)
        out_ref[:, number * part : (number + 1) * part] = combined.astype(BF16)

    for copy in to_across + to_mate + relayed + head_copies:
        copy.wait_send()

    def drain(step, carry):
        row_copy(step).wait_send()
        for number in range(CHUNKS):
            back_copy(number, step).wait_send()
        return carry

    lax.fori_loop(1, n, drain, 0)

    def drain_kv(step, carry):
        for copy in kv_copies(step, True):
            copy.wait_send()
        return carry

    lax.fori_loop(0, half, drain_kv, 0)

    def drain_outer(step, carry):
        for copy in kv_copies(step, False):
            copy.wait_send()
        return carry

    lax.fori_loop(1, half, drain_outer, 0)


def local(
    n,
    tp,
    query_rows,
    key_rows,
    value_rows,
    lambdas,
    head_gain,
    w_out,
    moe_rows,
    ffn_gain,
    routes,
    group_logits,
    pick_logits,
    w_gate,
    w_up,
    w_down,
):
    token_count = query_rows.shape[0]
    local_heads = lambdas.shape[1]
    head_qk = query_rows.shape[1] // (2 * local_heads)
    head_v = value_rows.shape[1] // local_heads
    width = moe_rows.shape[1]
    quarter = moe_rows.shape[0] // tp
    capacity = max(2, 2 * routes.shape[1] * quarter // n)
    units = w_gate.shape[2]
    part = width // CHUNKS
    share = token_count // tp
    dims = (token_count, local_heads, head_qk, head_v, quarter, capacity, group_logits.shape[1])
    vmem = pl.BlockSpec(memory_space=pltpu.VMEM)
    anywhere = pl.BlockSpec(memory_space=pl.ANY)
    dma = pltpu.SemaphoreType.DMA
    return pl.pallas_call(
        functools.partial(kernel, n, tp, dims),
        out_shape=(
            jax.ShapeDtypeStruct((share, width), BF16),
            jax.ShapeDtypeStruct((quarter, width), BF16),
        ),
        in_specs=[
            vmem,
            anywhere,
            anywhere,
            pl.BlockSpec(memory_space=pltpu.SMEM),
            vmem,
            anywhere,
            anywhere,
            vmem,
            vmem,
            vmem,
            vmem,
            anywhere,
            anywhere,
            anywhere,
        ],
        out_specs=(vmem, vmem),
        scratch_shapes=[
            pltpu.VMEM((quarter, width), BF16),
            pltpu.VMEM((n, capacity, width), BF16),
            pltpu.VMEM((n, capacity, width), BF16),
            pltpu.VMEM((4, width, units), BF16),
            pltpu.VMEM((4, width, units), BF16),
            pltpu.VMEM((4, units, width), BF16),
            pltpu.VMEM((n, token_count, key_rows.shape[1]), BF16),
            pltpu.VMEM((n, token_count, value_rows.shape[1]), BF16),
            pltpu.VMEM(w_out.shape, BF16),
            pltpu.VMEM((tp, share, local_heads * head_v), BF16),
            pltpu.VMEM((tp, share, local_heads * head_v), BF16),
            pltpu.VMEM((4, n * capacity, units), BF16),
            pltpu.VMEM((CHUNKS, n, capacity, part), BF16),
            pltpu.VMEM((CHUNKS, n, capacity, part), BF16),
            dma((7,)),
            dma((3, 2 + CHUNKS)),
            dma((3, 2 + CHUNKS)),
            dma((n,)),
            dma((n,)),
            dma((2, n)),
            dma((2, n)),
            dma((CHUNKS, n)),
            dma((CHUNKS, n)),
            dma((tp,)),
            dma((tp,)),
        ],
        compiler_params=pltpu.CompilerParams(
            collective_id=0, has_side_effects=True, vmem_limit_bytes=60 * 1024 * 1024
        ),
    )(
        query_rows,
        key_rows,
        value_rows,
        lambdas,
        head_gain.reshape(1, -1),
        w_out,
        moe_rows,
        ffn_gain.reshape(1, -1),
        routes,
        group_logits,
        pick_logits,
        w_gate,
        w_up,
        w_down,
    )


def solution(mesh):
    inner = jax.shard_map(
        functools.partial(local, mesh.shape["ep"], mesh.shape["tp"]),
        mesh=mesh,
        in_specs=(
            P("ep", "tp"),
            P("ep", "tp"),
            P("ep", "tp"),
            P(None, "tp"),
            P(),
            P(),
            P("ep", None),
            P(),
            P("ep", None),
            P("ep", None),
            P("ep", None),
            P("ep", None, "tp"),
            P("ep", None, "tp"),
            P("ep", "tp", None),
        ),
        out_specs=(P(("ep", "tp"), None), P(("ep", "tp"), None)),
        check_vma=False,
    )

    def whole(query_rows, key_rows, value_rows, lambdas, *rest):
        return inner(query_rows, key_rows, value_rows, lambdas.reshape(1, -1), *rest)

    return whole
```

time: 340 us -> 129 us (0.38)
  blocking collectives: 160 us -> 0 us
  Pallas kernels: 0 us -> 120 us
  waiting for transfers between devices: 107 us -> 0 us
  matrix products: 26.4 us -> 0 us
  between operations: 14 us -> 0.64 us
  other arithmetic: 10 us -> 0 us
  local copies, waits for them, and re-layouts: 16.6 us -> 8.12 us
  starting transfers between devices: 5.81 us -> 0 us
    pallas_call x0 -> x1, Pallas kernels: none -> 120 us  [local(): pl.pallas_call(functools.partial(kernel, n, tp, dims), out_shape=(jax.Sha...]
    all_gather x2 -> x0, blocking collectives: 104 us -> none  [the longest x1 71.9 us: local(): value_piece = lax.all_gather(value_rows, 'ep', axis=0, tiled=True)]
    all_gather x1 -> x0, waiting for transfers between devices: 57.2 us -> none  [local(): pieces = lax.all_gather(arrived, 'tp', axis=0, tiled=True)]
    all_to_all x1 -> x0, blocking collectives: 55.4 us -> none  [local(): lax.all_to_all(outgoing.reshape(expert_count, capacity, model_width), 'ep...]
    reduce_scatter x2 -> x0, waiting for transfers between devices: 49.9 us -> none  [the longest x1 37 us: local(): lax.psum_scatter(jnp.dot(hidden_flat, w_down[0], preferred_element_type=j...]
    dot_general x5 -> x0, matrix products: 26.4 us -> none  [the longest x1 13.2 us: local(): jnp.dot(hidden_flat, w_down[0], preferred_element_type=jnp.float32)]
    unnamed x21 -> x5, local copies, waits for them, and re-layouts: 1.2 us -> 8.12 us
    reduce_sum x8 -> x0, other arithmetic: 6.46 us -> none  [the longest x1 3.93 us: local(): jnp.sum(gate_values[..., None] * picked.astype(jnp.float32), axis=1)]
  transfers between devices with their start and end apart: 4 -> 0, of which waited for: 3 -> 0; matrix products, arithmetic and copies ran while one was open for 6% -> 0% of each run, Pallas kernels for 0% -> 0%
where the time goes in v1:
time: 129 us
  Pallas kernels  120 us (93%)
  local copies, waits for them, and re-layouts  8.12 us (6%)
    pallas_call x1, Pallas kernels, local(): pl.pallas_call(functools.partial(kernel, n, tp, dims), out_shape=(jax.Sha...  120 us
    unnamed x5, local copies, waits for them, and re-layouts  8.12 us

profile of v1, /device:TPU:0, one launch (start us, length us, event | category | flops | bytes accessed | tf_op | source)
XLA Modules:
  0.0 128.6 jit_solution(3448088377740883191)
XLA Ops:
  0.6 1.5 %copy.16.routes_ref = s32[512,2]{1,0:T(8,128)} copy(s32[512,2]{0,1:T(2,128)} %param.22) | data formatting | bytes 8192 | tf_op args[8]
  2.2 1.5 %copy.17.groups_ref = f32[512,4]{1,0:T(8,128)} copy(f32[512,4]{0,1:T(4,128)} %param.23) | data formatting | bytes 16384 | tf_op args[9]
  3.7 1.5 %copy.18.picks_ref = f32[512,2]{1,0:T(8,128)} copy(f32[512,2]{0,1:T(2,128)} %param.24) | data formatting | bytes 8192 | tf_op args[10]
  5.3 119.8 %shard_map.149 = (bf16[48,2048]{1,0:T(8,128)(2,1)}, bf16[128,2048]{1,0:T(8,128)(2,1)}) custom-call(bf16[192,256]{1,0:T(8,128)(2,1)} %query_ref.1, bf16[192,256]{1,0:T(8,128)(2,1)} %key_ref.1, bf16[192,256]{1,0:T(8,128)(2,1)} %value_ref.1, f32[1,2]{1,0:T(1,128)} %bitcast.4, f32[1,128]{1,0:T(1,128)} %bitcast.5, bf16[1024,2048]{1,0:T(8,128)(2,1)} %w_out_ref.1, ...), custom_call_target="tpu_custom_call" | custom-call | tf_op jit(solution)/shard_map/pallas_call | solution.py:477
  125.1 1.6 %copy.21 = bf16[48,2048]{1,0:T(8,128)(2,1)} copy(bf16[48,2048]{1,0:T(8,128)(2,1)} %get-tuple-element.4) | data formatting | bytes 393216
  126.7 1.9 %copy.22 = bf16[128,2048]{1,0:T(8,128)(2,1)} copy(bf16[128,2048]{1,0:T(8,128)(2,1)} %get-tuple-element.5) | data formatting | bytes 1048576

commit v2 on v1

--- a/solution.py
+++ b/solution.py
@@ -50,6 +50,8 @@
     mixer_ref,
     out_ref,
     rows_buf,
+    marks,
+    line,
     sent,
     arrived,
     w_gate,
@@ -64,6 +66,8 @@
     results,
     returned,
     local_sem,
+    line_send,
+    line_recv,
     weight_send,
     weight_recv,
     row_send,
@@ -83,6 +87,7 @@
     diagonal = lax.rem(mate + tp // 2, tp)
     beside = ep + 1 - 2 * lax.rem(ep, 2)
     half = n // 2
+    at, side = ep // 2, lax.rem(ep, 2)
     width = out_ref.shape[1]
     part = width // CHUNKS
 
@@ -104,8 +109,8 @@
         pltpu.make_async_copy(gate_ref.at[0], w_gate.at[0], local_sem.at[1]),
         pltpu.make_async_copy(up_ref.at[0], w_up.at[0], local_sem.at[2]),
         pltpu.make_async_copy(down_ref.at[0], w_down.at[0], local_sem.at[3]),
-        pltpu.make_async_copy(key_ref, keys.at[0], local_sem.at[4]),
-        pltpu.make_async_copy(value_ref, values.at[0], local_sem.at[5]),
+        pltpu.make_async_copy(key_ref, keys.at[ep], local_sem.at[4]),
+        pltpu.make_async_copy(value_ref, values.at[ep], local_sem.at[5]),
         pltpu.make_async_copy(w_out_ref, w_out, local_sem.at[6]),
     ]
     for copy in locals_:
@@ -172,90 +177,192 @@
         copy.start()
 
     own = pl.ds(pl.multiple_of(me * quarter, quarter), quarter)
-    routes = routes_ref[own, :]
-    first, second = routes[:, 0:1], routes[:, 1:2]
-    lanes = lax.broadcasted_iota(jnp.int32, (quarter, 128), 1)
-    away = [lax.rem(pick - ep + n, n) for pick in (first, second)]
-    named = jnp.where((lanes == away[0]) | (lanes == away[1]), 1.0, 0.0)
+    routes = routes_ref[:, own]
+    first, second = routes[0:1, :], routes[1:2, :]
+    experts = lax.broadcasted_iota(jnp.int32, (n, quarter), 0)
+    named = jnp.where((experts == first) | (experts == second), 1.0, 0.0)
     row_at = lax.broadcasted_iota(jnp.int32, (quarter, quarter), 0)
     column_at = lax.broadcasted_iota(jnp.int32, (quarter, quarter), 1)
-    earlier = jnp.where(column_at < row_at, 1.0, 0.0).astype(BF16)
-    before = jnp.dot(earlier, named.astype(BF16), preferred_element_type=F32)
-    places = [
-        away_k * capacity
-        + jnp.sum(jnp.where(lanes == away_k, before, 0.0), axis=1, keepdims=True).astype(jnp.int32)
-        for away_k in away
+    earlier = jnp.where(row_at < column_at, 1.0, 0.0).astype(BF16)
+    before = jnp.dot(named.astype(BF16), earlier, preferred_element_type=F32)
+    slots = [
+        (pick * capacity).astype(F32)
+        + jnp.sum(jnp.where(experts == pick, before, 0.0), axis=0, keepdims=True)
+        for pick in (first, second)
     ]
-    slot_at = lax.broadcasted_iota(jnp.int32, (quarter, n * capacity), 1)
-    pick_of = [jnp.where(slot_at == place, 1.0, 0.0) for place in places]
-    spread = (pick_of[0] + pick_of[1]).astype(BF16)
+    mark_at = lax.broadcasted_iota(jnp.int32, (8, quarter), 0)
+    marks[at] = jnp.where(mark_at == 0, slots[0], slots[1])
 
     own_rows.wait()
     tokens = rows_buf[...].astype(F32)
     squared = jnp.mean(tokens * tokens, axis=-1, keepdims=True)
-    normed = (tokens * lax.rsqrt(squared + EPS) * ffn_gain_ref[...]).astype(BF16)
-    slotted = lax.dot_general(
-        spread, normed, (((0,), (0,)), ((), ())), preferred_element_type=F32
-    )
-    sent[...] = split_rows(slotted, capacity)
-
-    def row_copy(step):
+    line[at] = (tokens * lax.rsqrt(squared + EPS) * ffn_gain_ref[...]).astype(BF16)
+
+    def line_copies(which, source, up):
+        device = (ep + 2 if up else ep - 2, me)
+        way = 0 if up else 1
+        pairs = (
+            ((marks.at[source], marks.at[source]), (line.at[source], line.at[source]))
+            if which == 0
+            else (
+                (keys.at[2 * source + side], keys.at[2 * source + side]),
+                (values.at[2 * source + side], values.at[2 * source + side]),
+            )
+        )
+        return [
+            remote(
+                pair[0],
+                pair[1],
+                line_send.at[which, k, way, source],
+                line_recv.at[which, k, source],
+                device,
+            )
+            for k, pair in enumerate(pairs)
+        ]
+
+    def send_on(which, source):
+        @pl.when(at + 1 < half)
+        def _():
+            for copy in line_copies(which, source, True):
+                copy.start()
+
+        @pl.when(at >= 1)
+        def _():
+            for copy in line_copies(which, source, False):
+                copy.start()
+
+    def walk(which, use):
+        def step_of(step, carry):
+            @pl.when(at - step >= 0)
+            def _():
+                source = at - step
+                for copy in line_copies(which, source, True):
+                    copy.wait_recv()
+
+                @pl.when(at + 1 < half)
+                def _():
+                    for copy in line_copies(which, source, True):
+                        copy.start()
+
+                use(source)
+
+            @pl.when(at + step < half)
+            def _():
+                source = at + step
+                for copy in line_copies(which, source, False):
+                    copy.wait_recv()
+
+                @pl.when(at >= 1)
+                def _():
+                    for copy in line_copies(which, source, False):
+                        copy.start()
+
+                use(source)
+
+            return carry
+
+        lax.fori_loop(1, half, step_of, 0)
+
+    def walk_drain(which):
+        def step_of(step, carry):
+            @pl.when((at - step >= 0) & (at + 1 < half))
+            def _():
+                for copy in line_copies(which, at - step, True):
+                    copy.wait_send()
+
+            @pl.when((at + step < half) & (at >= 1))
+            def _():
+                for copy in line_copies(which, at + step, False):
+                    copy.wait_send()
+
+            return carry
+
+        lax.fori_loop(1, half, step_of, 0)
+
+        @pl.when(at + 1 < half)
+        def _():
+            for copy in line_copies(which, at, True):
+                copy.wait_send()
+
+        @pl.when(at >= 1)
+        def _():
+            for copy in line_copies(which, at, False):
+                copy.wait_send()
+
+    def side_rows(source):
         return remote(
-            sent.at[step],
-            arrived.at[step],
-            row_send.at[step],
-            row_recv.at[step],
-            (lax.rem(ep + step, n), me),
-        )
-
-    def start_rows(step, carry):
-        row_copy(step).start()
-        return carry
-
-    lax.fori_loop(1, n, start_rows, 0)
-    arrived[0] = sent[0]
-
-    def kv_copies(step, relay):
-        to = step + half if relay else step
-        device = (beside, me) if relay else (lax.rem(ep + 2 * step, n), me)
-        key_source = keys.at[step] if relay else key_ref
-        value_source = values.at[step] if relay else value_ref
-        return (
-            remote(key_source, keys.at[to], kv_send.at[0, to], kv_recv.at[0, to], device),
-            remote(value_source, values.at[to], kv_send.at[1, to], kv_recv.at[1, to], device),
-        )
-
-    def start_kv(step, carry):
-        for copy in kv_copies(step, False):
+            sent.at[source],
+            arrived.at[2 * source + side],
+            row_send.at[source],
+            row_recv.at[source],
+            (beside, me),
+        )
+
+    slot_at = lax.broadcasted_iota(jnp.int32, (capacity, quarter), 0)
+
+    def select(source):
+        mark = marks[source].astype(jnp.int32)
+        block = line[source]
+
+        def rows_of(expert):
+            place = slot_at + expert * capacity
+            spread = jnp.where((place == mark[0:1, :]) | (place == mark[1:2, :]), 1.0, 0.0)
+            return jnp.dot(spread.astype(BF16), block, preferred_element_type=F32).astype(BF16)
+
+        sent[source] = rows_of(beside)
+        side_rows(source).start()
+        arrived[2 * source + side] = rows_of(ep)
+
+    send_on(0, at)
+    select(at)
+
+    groups = groups_ref[:, own]
+    group_weights = jnp.exp(groups - jnp.max(groups, axis=0, keepdims=True))
+    group_prob = group_weights / jnp.sum(group_weights, axis=0, keepdims=True)
+    picks = picks_ref[:, own]
+    pick_weights = jnp.exp(picks - jnp.max(picks, axis=0, keepdims=True))
+    pick_prob = pick_weights / jnp.sum(pick_weights, axis=0, keepdims=True)
+    group_at = lax.broadcasted_iota(jnp.int32, groups.shape, 0)
+    gates = []
+    for k, pick in enumerate((first, second)):
+        gate_row = (
+            jnp.sum(
+                jnp.where(group_at == pick // (n // group_count), group_prob, 0.0),
+                axis=0,
+                keepdims=True,
+            )
+            * pick_prob[k : k + 1, :]
+        )
+        gates.append(
+            jnp.sum(jnp.where(row_at == column_at, gate_row, 0.0), axis=1, keepdims=True)
+        )
+
+    walk(0, select)
+
+    def side_kv(source):
+        place = 2 * source + side
+        return [
+            remote(keys.at[place], keys.at[place], kv_send.at[0, source], kv_recv.at[0, source], (beside, me)),
+            remote(values.at[place], values.at[place], kv_send.at[1, source], kv_recv.at[1, source], (beside, me)),
+        ]
+
+    def relay_kv(source):
+        for copy in side_kv(source):
             copy.start()
-        return carry
-
-    lax.fori_loop(1, half, start_kv, 0)
-
-    groups = groups_ref[own, :]
-    group_weights = jnp.exp(groups - jnp.max(groups, axis=-1, keepdims=True))
-    group_prob = group_weights / jnp.sum(group_weights, axis=-1, keepdims=True)
-    picks = picks_ref[own, :]
-    pick_weights = jnp.exp(picks - jnp.max(picks, axis=-1, keepdims=True))
-    pick_prob = pick_weights / jnp.sum(pick_weights, axis=-1, keepdims=True)
-    group_at = lax.broadcasted_iota(jnp.int32, groups.shape, 1)
-    gates = [
-        jnp.sum(jnp.where(group_at == pick // (n // group_count), group_prob, 0.0), axis=1, keepdims=True)
-        * pick_prob[:, k : k + 1]
-        for k, pick in enumerate((first, second))
-    ]
 
     for copy in locals_:
         copy.wait()
+    send_on(1, at)
+    relay_kv(at)
 
     to_across[0].wait_recv()
     relayed[0].start()
 
-    def wait_rows(step, carry):
-        row_copy(step).wait_recv()
+    def wait_rows(source, carry):
+        side_rows(source).wait_recv()
         return carry
 
-    lax.fori_loop(1, n, wait_rows, 0)
+    lax.fori_loop(0, half, wait_rows, 0)
     units = gate_ref.shape[2]
 
     def hide(place):
@@ -275,13 +382,17 @@
     relayed[1].wait_recv()
     hide(3)
 
-    def back_copy(number, step):
+    walk(1, relay_kv)
+
+    def back_copy(number, step, receive):
+        other = lax.rem(ep + step, n)
+        expert = other if receive else ep
         return remote(
-            results.at[number, step],
-            returned.at[number, step],
+            results.at[number, other],
+            returned.at[number, expert],
             back_send.at[number, step],
-            back_recv.at[number, step],
-            (lax.rem(ep - step + n, n), me),
+            back_recv.at[number, expert],
+            (other, me),
         )
 
     for number in range(CHUNKS):
@@ -298,25 +409,14 @@
         results[number] = split_rows(total, capacity)
 
         def start_back(step, carry):
-            back_copy(number, step).start()
+            back_copy(number, step, False).start()
             return carry
 
         lax.fori_loop(1, n, start_back, 0)
-        returned[number, 0] = results[number, 0]
-
-    def relay_kv(step, carry):
-        for copy in kv_copies(step, False):
-            copy.wait_recv()
-        for copy in kv_copies(step, True):
-            copy.start()
-        return carry
-
-    for copy in kv_copies(0, True):
-        copy.start()
-    lax.fori_loop(1, half, relay_kv, 0)
-
-    def wait_kv(step, carry):
-        for copy in kv_copies(step, True):
+        returned[number, ep] = results[number, ep]
+
+    def wait_kv(source, carry):
+        for copy in side_kv(source):
             copy.wait_recv()
         return carry
 
@@ -328,11 +428,11 @@
     for head in range(local_heads):
         averaged = []
         for way in range(2):
-            at = (2 * head + way) * head_qk
-            query = query_ref[:, at : at + head_qk]
+            column = (2 * head + way) * head_qk
+            query = query_ref[:, column : column + head_qk]
 
             def scored(step):
-                key_rows = keys[pl.ds(step * blocks, blocks), :, at : at + head_qk]
+                key_rows = keys[pl.ds(step * blocks, blocks), :, column : column + head_qk]
                 return (
                     lax.dot_general(
                         query,
@@ -403,43 +503,46 @@
         )
     mixer_ref[...] = mixed.astype(BF16)
 
-    choose = [pick.astype(BF16) for pick in pick_of]
+    back_at = lax.broadcasted_iota(jnp.int32, (n * capacity, quarter), 0)
+    choose = [
+        jnp.where(back_at == slot.astype(jnp.int32), 1.0, 0.0).astype(BF16) for slot in slots
+    ]
+    over_rows = (((0,), (0,)), ((), ()))
     for number in range(CHUNKS):
 
         def wait_back(step, carry):
-            back_copy(number, step).wait_recv()
+            back_copy(number, step, True).wait_recv()
             return carry
 
         lax.fori_loop(1, n, wait_back, 0)
         rows = flat_rows(returned[number])
-        combined = gates[0] * jnp.dot(choose[0], rows, preferred_element_type=F32)
-        combined += gates[1] * jnp.dot(choose[1], rows, preferred_element_type=F32)
+        combined = gates[0] * lax.dot_general(
+            choose[0], rows, over_rows, preferred_element_type=F32
+        )
+        combined += gates[1] * lax.dot_general(
+            choose[1], rows, over_rows, preferred_element_type=F32
+        )
         out_ref[:, number * part : (number + 1) * part] = combined.astype(BF16)
 
     for copy in to_across + to_mate + relayed + head_copies:
         copy.wait_send()
 
     def drain(step, carry):
-        row_copy(step).wait_send()
         for number in range(CHUNKS):
-            back_copy(number, step).wait_send()
+            back_copy(number, step, False).wait_send()
         return carry
 
     lax.fori_loop(1, n, drain, 0)
 
-    def drain_kv(step, carry):
-        for copy in kv_copies(step, True):
+    def drain_side(source, carry):
+        side_rows(source).wait_send()
+        for copy in side_kv(source):
             copy.wait_send()
         return carry
 
-    lax.fori_loop(0, half, drain_kv, 0)
-
-    def drain_outer(step, carry):
-        for copy in kv_copies(step, False):
-            copy.wait_send()
-        return carry
-
-    lax.fori_loop(1, half, drain_outer, 0)
+    lax.fori_loop(0, half, drain_side, 0)
+    walk_drain(0)
+    walk_drain(1)
 
 
 def local(
@@ -466,11 +569,11 @@
     head_v = value_rows.shape[1] // local_heads
     width = moe_rows.shape[1]
     quarter = moe_rows.shape[0] // tp
-    capacity = max(2, 2 * routes.shape[1] * quarter // n)
+    capacity = max(2, 2 * routes.shape[0] * quarter // n)
     units = w_gate.shape[2]
     part = width // CHUNKS
     share = token_count // tp
-    dims = (token_count, local_heads, head_qk, head_v, quarter, capacity, group_logits.shape[1])
+    dims = (token_count, local_heads, head_qk, head_v, quarter, capacity, group_logits.shape[0])
     vmem = pl.BlockSpec(memory_space=pltpu.VMEM)
     anywhere = pl.BlockSpec(memory_space=pl.ANY)
     dma = pltpu.SemaphoreType.DMA
@@ -499,7 +602,9 @@
         out_specs=(vmem, vmem),
         scratch_shapes=[
             pltpu.VMEM((quarter, width), BF16),
-            pltpu.VMEM((n, capacity, width), BF16),
+            pltpu.VMEM((n // 2, 8, quarter), F32),
+            pltpu.VMEM((n // 2, quarter, width), BF16),
+            pltpu.VMEM((n // 2, capacity, width), BF16),
             pltpu.VMEM((n, capacity, width), BF16),
             pltpu.VMEM((4, width, units), BF16),
             pltpu.VMEM((4, width, units), BF16),
@@ -513,12 +618,14 @@
             pltpu.VMEM((CHUNKS, n, capacity, part), BF16),
             pltpu.VMEM((CHUNKS, n, capacity, part), BF16),
             dma((7,)),
+            dma((2, 2, 2, n // 2)),
+            dma((2, 2, n // 2)),
             dma((3, 2 + CHUNKS)),
             dma((3, 2 + CHUNKS)),
-            dma((n,)),
-            dma((n,)),
-            dma((2, n)),
-            dma((2, n)),
+            dma((n // 2,)),
+            dma((n // 2,)),
+            dma((2, n // 2)),
+            dma((2, n // 2)),
             dma((CHUNKS, n)),
             dma((CHUNKS, n)),
             dma((tp,)),
@@ -558,9 +665,9 @@
             P(),
             P("ep", None),
             P(),
-            P("ep", None),
-            P("ep", None),
-            P("ep", None),
+            P(None, "ep"),
+            P(None, "ep"),
+            P(None, "ep"),
             P("ep", None, "tp"),
             P("ep", None, "tp"),
             P("ep", "tp", None),
@@ -569,7 +676,11 @@
         check_vma=False,
     )
 
-    def whole(query_rows, key_rows, value_rows, lambdas, *rest):
-        return inner(query_rows, key_rows, value_rows, lambdas.reshape(1, -1), *rest)
+    def whole(*args):
+        args = list(args)
+        args[3] = args[3].reshape(1, -1)
+        for place in (8, 9, 10):
+            args[place] = args[place].T
+        return inner(*args)
 
     return whole

time: 129 us -> 118 us (0.915)
  Pallas kernels: 120 us -> 112 us
  local copies, waits for them, and re-layouts: 8.12 us -> 3.5 us
    pallas_call x1, Pallas kernels: 120 us -> 112 us  [local(): pl.pallas_call(functools.partial(kernel, n, tp, dims), out_shape=(jax.Sha...]
    unnamed x5 -> x2, local copies, waits for them, and re-layouts: 8.12 us -> 3.5 us
where the time goes in v2:
time: 118 us; the launch traced here: 117 us
  Pallas kernels  112 us (95%)
  local copies, waits for them, and re-layouts  3.5 us (3%)
    pallas_call x1, Pallas kernels, local(): pl.pallas_call(functools.partial(kernel, n, tp, dims), out_shape=(jax.Sha...  112 us
    unnamed x2, local copies, waits for them, and re-layouts  3.5 us

profile of v2, /device:TPU:0, one launch (start us, length us, event | category | flops | bytes accessed | tf_op | source)
XLA Modules:
  0.0 116.6 jit_solution(13999261005045537889)
XLA Ops:
  0.6 112.4 %shard_map.149 = (bf16[48,2048]{1,0:T(8,128)(2,1)}, bf16[128,2048]{1,0:T(8,128)(2,1)}) custom-call(bf16[192,256]{1,0:T(8,128)(2,1)} %query_ref.1, bf16[192,256]{1,0:T(8,128)(2,1)} %key_ref.1, bf16[192,256]{1,0:T(8,128)(2,1)} %value_ref.1, f32[1,2]{1,0:T(1,128)} %bitcast.10, f32[1,128]{1,0:T(1,128)} %bitcast.11, bf16[1024,2048]{1,0:T(8,128)(2,1)} %w_out_ref.1, ...), custom_call_target="tpu_custom_call" | custom-call | tf_op jit(solution)/shard_map/pallas_call | solution.py:580
  113.1 1.6 %copy.18 = bf16[48,2048]{1,0:T(8,128)(2,1)} copy(bf16[48,2048]{1,0:T(8,128)(2,1)} %get-tuple-element.4) | data formatting | bytes 393216
  114.7 1.9 %copy.19 = bf16[128,2048]{1,0:T(8,128)(2,1)} copy(bf16[128,2048]{1,0:T(8,128)(2,1)} %get-tuple-element.5) | data formatting | bytes 1048576

commit v3 on v2

--- a/solution.py
+++ b/solution.py
@@ -9,7 +9,7 @@
 
 EPS = 1e-06
 HEAD_SCALE = 0.8
-CHUNKS = 4
+CHUNKS = 8
 MESH = pl.DeviceIdType.MESH
 F32 = jnp.float32
 BF16 = jnp.bfloat16
@@ -545,6 +545,11 @@
     walk_drain(1)
 
 
+def hand_over(mixed_ref, combined_ref, mixer_ref, out_ref):
+    mixer_ref[...] = mixed_ref[...]
+    out_ref[...] = combined_ref[...]
+
+
 def local(
     n,
     tp,
@@ -577,7 +582,7 @@
     vmem = pl.BlockSpec(memory_space=pltpu.VMEM)
     anywhere = pl.BlockSpec(memory_space=pl.ANY)
     dma = pltpu.SemaphoreType.DMA
-    return pl.pallas_call(
+    mixed, combined = pl.pallas_call(
         functools.partial(kernel, n, tp, dims),
         out_shape=(
             jax.ShapeDtypeStruct((share, width), BF16),
@@ -650,6 +655,16 @@
         w_up,
         w_down,
     )
+    return pl.pallas_call(
+        hand_over,
+        out_shape=(
+            jax.ShapeDtypeStruct(mixed.shape, BF16),
+            jax.ShapeDtypeStruct(combined.shape, BF16),
+        ),
+        in_specs=[vmem, vmem],
+        out_specs=(vmem, vmem),
+        compiler_params=pltpu.CompilerParams(vmem_limit_bytes=8 * 1024 * 1024),
+    )(mixed, combined)
 
 
 def solution(mesh):

time: 118 us -> 119 us (level)
  Pallas kernels: 112 us -> 116 us
  local copies, waits for them, and re-layouts: 3.5 us -> 1.96 us
    pallas_call x1, Pallas kernels: 112 us -> 115 us  [local(): pl.pallas_call(functools.partial(kernel, n, tp, dims), out_shape=(jax.Sha...]
    unnamed x2 -> x4, local copies, waits for them, and re-layouts: 3.5 us -> 1.96 us
where the time goes in v3:
time: 119 us; the launch traced here: 118 us
  Pallas kernels  116 us (97%)
  local copies, waits for them, and re-layouts  1.96 us (2%)
    pallas_call x1, Pallas kernels, local(): pl.pallas_call(functools.partial(kernel, n, tp, dims), out_shape=(jax.Sha...  115 us

profile of v3, /device:TPU:0, one launch (start us, length us, event | category | flops | bytes accessed | tf_op | source)
XLA Modules:
  0.0 118.4 jit_solution(3770048206305229789)
XLA Ops:
  0.6 114.8 %shard_map.149 = (bf16[48,2048]{1,0:T(8,128)(2,1)}, bf16[128,2048]{1,0:T(8,128)(2,1)}) custom-call(bf16[192,256]{1,0:T(8,128)(2,1)} %query_ref.1, bf16[192,256]{1,0:T(8,128)(2,1)} %key_ref.1, bf16[192,256]{1,0:T(8,128)(2,1)} %value_ref.1, f32[1,2]{1,0:T(1,128)} %bitcast.10, f32[1,128]{1,0:T(1,128)} %bitcast.11, bf16[1024,2048]{1,0:T(8,128)(2,1)} %w_out_ref.1, ...), custom_call_target="tpu_custom_call" | custom-call | tf_op jit(solution)/shard_map/pallas_call | solution.py:585
  115.5 0.0 copy-start
  115.5 1.0 copy-done
  116.5 0.0 copy-start.1
  116.5 0.9 copy-done.1
  117.5 0.9 shard_map.150
Async XLA Ops:
  115.5 1.0 copy-start
  116.5 0.9 copy-start.1
